TPU v7x, 32 devices: a whole 2x2x4 slice. The times are simulated.
32 devices in a mesh: rep: 2 (over x), fs: 8 (over z, y), tp: 2 (over core).
Axes of the slice: x: 2, y: 2, z: 4, core: 2. Of those that a mesh axis runs over, the one named last changes fastest.
Arguments:
- inputs: bfloat16 [8192, 2048], P(('rep', 'fs')), may hold values from -6 to 6
- gain: float32 [2048], replicated, may hold values from 0.1 to 1.9
- gate_weight: bfloat16 [2048, 3072], P('fs', 'tp'), may hold values from -0.125 to 0.125
- up_weight: bfloat16 [2048, 3072], P('fs', 'tp'), may hold values from -0.125 to 0.125
- down_weight: bfloat16 [2048, 3072], P('fs', 'tp'), may hold values from -0.109375 to 0.109375
- cotangent: bfloat16 [8192, 2048], P(('rep', 'fs')), may hold values from -6 to 6
Outputs:
- input_gradient: bfloat16 [8192, 2048], P(('rep', 'fs'))
- gain_gradient: float32 [2048], replicated
- d_down: float32 [2048, 3072], P('fs', 'tp')
All inputs are finite; a program needn't handle non-finite values.
Results may differ from a plain program's by a relative error of at most 0.014.
Values may be sent and summed in bfloat16 or wider, within the bound.
A program may use at most 128 MiB of HBM per device.

v0:
```python
import jax
import jax.numpy as jnp
from jax import lax
from jax.sharding import PartitionSpec as P

EPS = 1e-06


def local(inputs, gain, gate_weight, up_weight, down_weight, cotangent):
    single_precision = inputs.astype(jnp.float32)
    reciprocal_root_mean = lax.rsqrt(
        jnp.mean(single_precision * single_precision, axis=-1, keepdims=True) + EPS
    )
    unit_input = single_precision * reciprocal_root_mean
    normalized_input = (unit_input * gain).astype(jnp.bfloat16)
    row_count = inputs.shape[0]
    contract_cols = (((1,), (1,)), ((), ()))
    gate_full, up_full, down_full = (
        lax.all_gather(gate_weight, "fs", axis=0, tiled=True),
        lax.all_gather(up_weight, "fs", axis=0, tiled=True),
        lax.all_gather(down_weight, "fs", axis=0, tiled=True),
    )
    gate = jnp.dot(normalized_input, gate_full, preferred_element_type=jnp.float32)
    up_proj = jnp.dot(normalized_input, up_full, preferred_element_type=jnp.float32)
    down_sum = jnp.dot(cotangent, down_full, preferred_element_type=jnp.float32)
    gate_sig = jax.nn.sigmoid(gate)
    active = gate * gate_sig
    hidden = (active * up_proj).astype(jnp.bfloat16)
    d_hidden = 0.5 * down_sum
    d_gate = (d_hidden * up_proj * gate_sig * (1.0 + gate * (1.0 - gate_sig))).astype(jnp.bfloat16)
    d_up = (d_hidden * active).astype(jnp.bfloat16)
    partial_value = lax.dot_general(
        d_gate, gate_full, contract_cols, preferred_element_type=jnp.float32
    ) + lax.dot_general(d_up, up_full, contract_cols, preferred_element_type=jnp.float32)
    summed_units = lax.psum(partial_value.astype(jnp.bfloat16), "tp")
    normalized_gradient = summed_units.astype(jnp.float32)
    gain_gradient = lax.psum(jnp.sum(normalized_gradient * unit_input, axis=0), ("rep", "fs"))
    gain_scaled = gain * normalized_gradient
    mean_correction = jnp.mean(gain_scaled * unit_input, axis=-1, keepdims=True)
    input_gradient = (
        cotangent.astype(jnp.float32)
        + reciprocal_root_mean * (gain_scaled - unit_input * mean_correction)
    ).astype(jnp.bfloat16)
    contract_rows = (((0,), (0,)), ((), ()))
    width = cotangent.shape[1]
    groups_fs = lax.axis_size("fs")
    groups_rep = lax.axis_size("rep")
    sub_rows = width // (groups_fs * groups_rep)
    reordered = (
        cotangent.reshape(row_count, groups_fs, groups_rep, sub_rows)
        .transpose(0, 2, 1, 3)
        .reshape(row_count, width)
    )
    summed = lax.psum_scatter(
        0.5 * lax.dot_general(reordered, hidden, contract_rows, preferred_element_type=jnp.float32),
        ("rep", "fs"),
        scatter_dimension=0,
        tiled=True,
    )
    d_down = lax.all_gather(summed, "rep", axis=0, tiled=True)
    return (input_gradient, gain_gradient, d_down)


def solution(mesh):
    placed = (
        P(("rep", "fs"), None),
        P(),
        P("fs", "tp"),
        P("fs", "tp"),
        P("fs", "tp"),
        P(("rep", "fs"), None),
    )
    return jax.shard_map(
        local,
        mesh=mesh,
        in_specs=placed,
        out_specs=(P(("rep", "fs"), None), P(), P("fs", "tp")),
        check_vma=False,
    )
```

profile of v0, /device:TPU:0, one launch (start us, length us, event | category | flops | bytes accessed | tf_op | source)
XLA Modules:
  0.0 600.7 jit_solution(4841965839708579481)
XLA Ops:
  7.2 0.7 all-gather.9.cloned.1.call-update
  8.0 0.7 all-gather.7.cloned.1.call-update
  8.7 0.7 all-gather.5.cloned.1.call-update
  9.5 2.5 copy.11
  12.0 3.3 copy.12
  15.2 0.5 fusion.9
  15.7 95.9 %all-gather.9.cloned.1.call-done = bf16[2048,1536]{1,0:T(8,128)(2,1)} async-done(((bf16[256,1536]{1,0:T(8,128)(2,1)}), bf16[2048,1536]{1,0:T(8,128)(2,1)}) %all-gather.9.cloned.1.call-update) | async-done | bytes 6291472 | tf_op jit(solution)/shard_map/all_gather | solution.py:19
  111.6 7.9 %fusion.14 = f32[512,1536]{1,0:T(8,128)} fusion(bf16[2048,1536]{1,0:T(8,128)(2,1)} %all-gather.9.cloned.1.call-done, bf16[512,2048]{1,0:T(8,128)(2,1)S(1)} %copy-done, f32[2048]{0:T(1024)S(1)} %copy-done.3, f32[512]{0:T(512)S(1)} %add_rsqrt_fusion), kind=kOutput, calls=%fused_computation.25 | convolution fusion | flops 3225419776 | bytes 11544576 | tf_op jit(solution)/shard_map/dot_general | solution.py:23
  119.5 91.2 %all-gather.7.cloned.1.call-done = bf16[2048,1536]{1,0:T(8,128)(2,1)} async-done(((bf16[256,1536]{1,0:T(8,128)(2,1)}), bf16[2048,1536]{1,0:T(8,128)(2,1)}) %all-gather.7.cloned.1.call-update) | async-done | bytes 6291472 | tf_op jit(solution)/shard_map/all_gather | solution.py:20
  210.7 5.8 fusion.16
  216.5 1.7 copy-done.6
  218.2 6.8 %multiply_bitcast_fusion = f32[2048,1536]{0,1:T(8,128)} fusion(bf16[512,2048]{0,1:T(8,128)(2,1)S(1)} %bitcast.14, f32[512,1536]{1,0:T(8,128)S(1)} %fusion.16, f32[512,1536]{1,0:T(8,128)S(1)} %copy-done.4), kind=kOutput, calls=%fused_computation | convolution fusion | flops 3229089792 | bytes 20971520 | tf_op jit(solution)/shard_map/dot_general | solution.py:55
  225.1 0.2 all-reduce.2.cloned.1.call-start
  225.3 84.5 %all-gather.5.cloned.1.call-done = bf16[2048,1536]{1,0:T(8,128)(2,1)} async-done(((bf16[256,1536]{1,0:T(8,128)(2,1)}), bf16[2048,1536]{1,0:T(8,128)(2,1)}) %all-gather.5.cloned.1.call-update) | async-done | bytes 6291472 | tf_op jit(solution)/shard_map/all_gather | solution.py:21
  309.8 8.6 %convolution_multiply_fusion = f32[512,1536]{1,0:T(8,128)} fusion(bf16[512,2048]{1,0:T(8,128)(2,1)} %param.11, bf16[2048,1536]{1,0:T(8,128)(2,1)} %all-gather.5.cloned.1.call-done), kind=kOutput, calls=%fused_computation.17 | convolution fusion | flops 3222011904 | bytes 11534336 | tf_op jit(solution)/shard_map/dot_general | solution.py:25
  318.4 8.6 %fusion.12 = f32[512,2048]{1,0:T(8,128)S(1)} fusion(bf16[2048,1536]{1,0:T(8,128)(2,1)} %all-gather.9.cloned.1.call-done, f32[512,1536]{1,0:T(8,128)S(1)} %copy-done.5, f32[512,1536]{1,0:T(8,128)} %convolution_multiply_fusion, f32[512,1536]{1,0:T(8,128)S(1)} %copy-done.7), kind=kOutput, calls=%fused_computation.23 | convolution fusion | flops 3229089792 | bytes 19922944 | tf_op jit(solution)/shard_map/dot_general | solution.py:32
  327.1 6.6 %add_convert_fusion = bf16[512,2048]{1,0:T(8,128)(2,1)} fusion(f32[512,2048]{1,0:T(8,128)S(1)} %fusion.12, bf16[2048,1536]{1,0:T(8,128)(2,1)S(1)} %bitcast.16, f32[512,1536]{1,0:T(8,128)} %convolution_multiply_fusion, f32[512,1536]{1,0:T(8,128)S(1)} %copy-done.5), kind=kOutput, calls=%fused_computation.16 | convolution fusion | flops 3228041216 | bytes 18874368 | tf_op jit(solution)/shard_map/dot_general | solution.py:34
  333.7 0.0 all-gather.11.cloned.1.call-start
  333.7 182.3 %reduce-scatter.2.cloned.1.call-done = f32[128,1536]{0,1:T(8,128)} async-done(((f32[2048,1536]{0,1:T(8,128)}), f32[128,1536]{0,1:T(8,128)}) %reduce-scatter.2.cloned.1.call-update) | async-done | bytes 786448 | tf_op jit(solution)/shard_map/reduce_scatter | solution.py:54
  516.1 23.6 %all-reduce.2.cloned.1.call-done = bf16[512,2048]{1,0:T(8,128)(2,1)} async-done(((bf16[512,2048]{1,0:T(8,128)(2,1)}), bf16[512,2048]{1,0:T(8,128)(2,1)}) %all-reduce.2.cloned.1.call-update) | async-done | bytes 2097168 | tf_op jit(solution)/shard_map/psum | solution.py:35
  539.6 2.9 fusion.10
  542.5 43.3 %psum.15 = f32[2048]{0:T(1024)} all-reduce(f32[2048]{0:T(1024)S(1)} %get-tuple-element.12), channel_id=1, replica_groups=mesh['rep'=2,'fs'=8,'tp'=2] {'rep','fs'}, use_global_device_ids=true, to_apply=%region_4.0 | all-reduce | flops 2048 | bytes 16384 | tf_op jit(solution)/shard_map/psum | solution.py:37
  585.8 5.0 fusion.6
  590.8 3.0 copy.13
  (30 shorter events, 0.3 us)
Async XLA Ops:
  7.2 2.3 copy-start.1
  7.2 104.4 %all-gather.9.cloned.1.call-start = ((), (), s32[]{:S(2)}) async-start(), calls=%async_computation.3 | async-start | bytes 7077888 | tf_op jit(solution)/shard_map/all_gather | solution.py:19
  7.9 202.8 %all-gather.7.cloned.1.call-start = ((), (), s32[]{:S(2)}) async-start(), calls=%async_computation.2 | async-start | bytes 7077888 | tf_op jit(solution)/shard_map/all_gather | solution.py:20
  8.7 301.1 %all-gather.5.cloned.1.call-start = ((), (), s32[]{:S(2)}) async-start(), calls=%async_computation.1 | async-start | bytes 7077888 | tf_op jit(solution)/shard_map/all_gather | solution.py:21
  9.4 506.6 %reduce-scatter.2.cloned.1.call-start = ((), (), s32[]{:S(2)}) async-start(), calls=%async_computation.5 | async-start | bytes 13369344 | tf_op jit(solution)/shard_map/reduce_scatter | solution.py:54
  12.0 3.3 copy-start
  12.0 99.7 %copy-start.3 = (f32[2048]{0:T(1024)S(1)}, f32[2048]{0:T(1024)}, u32[]{:S(2)}) copy-start(f32[2048]{0:T(1024)} %param.7) | copy-start | bytes 24580
  210.7 7.5 %copy-start.2 = (bf16[512,2,8,128]{0,3,2,1:T(8,128)(2,1)S(1)}, bf16[512,2,8,128]{0,3,2,1:T(8,128)(2,1)}, u32[]{:S(2)}) copy-start(bf16[512,2,8,128]{0,3,2,1:T(8,128)(2,1)} %copy.12) | copy-start | bytes 6291460
  210.7 7.5 %copy-start.4 = (f32[512,1536]{1,0:T(8,128)S(1)}, f32[512,1536]{1,0:T(8,128)}, u32[]{:S(2)}) copy-start(f32[512,1536]{1,0:T(8,128)} %fusion.14) | copy-start | bytes 9437188
  216.5 1.8 copy-start.6
  225.1 314.5 %all-reduce.2.cloned.1.call-start = ((), (), s32[]{:S(2)}) async-start(), calls=%async_computation.4 | async-start | bytes 4194304 | tf_op jit(solution)/shard_map/psum | solution.py:35
  309.8 8.6 %copy-start.5 = (f32[512,1536]{1,0:T(8,128)S(1)}, f32[512,1536]{1,0:T(8,128)}, u32[]{:S(2)}) copy-start(f32[512,1536]{1,0:T(8,128)} %fusion.14) | copy-start | bytes 9437188
  309.8 8.6 %copy-start.7 = (f32[512,1536]{1,0:T(8,128)S(1)}, f32[512,1536]{1,0:T(8,128)}, u32[]{:S(2)}) copy-start(f32[512,1536]{1,0:T(8,128)} %copy-done.6) | copy-start | bytes 9437188
  309.8 17.2 %slice-start = ((s8[6291456]{0:T(1024)(128)(4,1)}), s8[4194304]{0:T(1024)(128)(4,1)S(1)}, s32[]{:S(2)}) async-start(s8[6291456]{0:T(1024)(128)(4,1)} %bitcast.15), calls=%async_computation.7 | async-start | bytes 8388608
  318.4 8.6 %slice-start.1 = ((s8[6291456]{0:T(1024)(128)(4,1)}), s8[2097152]{0:T(1024)(128)(4,1)S(1)}, s32[]{:S(2)}) async-start(s8[6291456]{0:T(1024)(128)(4,1)} %bitcast.15), calls=%async_computation.8 | async-start | bytes 4194304
  333.7 257.1 %all-gather.11.cloned.1.call-start = ((), (), s32[]{:S(2)}) async-start(), calls=%async_computation.6 | async-start | bytes 2359296 | tf_op jit(solution)/shard_map/all_gather | solution.py:60
Sparse Core Ops, SparseCore 0:
  10.2 101.4 all-gather.8
  113.8 96.8 all-gather.6
  212.9 96.8 all-gather.4
  315.3 200.6 reduce-scatter.1
  518.8 20.7 all-reduce.1
  541.0 28.3 all-gather.10
where the time goes:
time: 601 us
  waiting for transfers between devices  480 us (80%)
  matrix products  44.2 us (7%)
  blocking collectives  43.3 us (7%)
  between operations  14.2 us (2%)
  local copies, waits for them, and re-layouts  10.6 us (2%)
  other arithmetic  8.39 us (1%)
    reduce_scatter x1, waiting for transfers between devices, local(): lax.psum_scatter(0.5 * lax.dot_general(reordered, hidden, contract_rows,...  182 us
    all_gather x1, waiting for transfers between devices, local(): lax.all_gather(gate_weight, 'fs', axis=0, tiled=True)  95.9 us
    all_gather x1, waiting for transfers between devices, local(): lax.all_gather(up_weight, 'fs', axis=0, tiled=True)  91.2 us
    all_gather x1, waiting for transfers between devices, local(): lax.all_gather(down_weight, 'fs', axis=0, tiled=True)  84.5 us
    psum x1, blocking collectives, local(): lax.psum(jnp.sum(normalized_gradient * unit_input, axis=0), ('rep', 'fs'))  43.3 us
    psum x1, waiting for transfers between devices, local(): summed_units = lax.psum(partial_value.astype(jnp.bfloat16), 'tp')  23.6 us
  transfers between devices with their start and end apart: 6, of which 5 were waited for; matrix products, arithmetic and copies ran while one was open for 10% of the time, Pallas kernels for 0%

commit v1 on v0

--- a/solution.py
+++ b/solution.py
@@ -34,7 +34,9 @@
     ) + lax.dot_general(d_up, up_full, contract_cols, preferred_element_type=jnp.float32)
     summed_units = lax.psum(partial_value.astype(jnp.bfloat16), "tp")
     normalized_gradient = summed_units.astype(jnp.float32)
-    gain_gradient = lax.psum(jnp.sum(normalized_gradient * unit_input, axis=0), ("rep", "fs"))
+    gain_gradient = lax.psum(
+        lax.psum(jnp.sum(normalized_gradient * unit_input, axis=0), "fs"), "rep"
+    )
     gain_scaled = gain * normalized_gradient
     mean_correction = jnp.mean(gain_scaled * unit_input, axis=-1, keepdims=True)
     input_gradient = (

time: 601 us -> 585 us (0.973)
  blocking collectives: 43.3 us -> 27.5 us
    psum x1 -> x2, blocking collectives: 43.3 us -> 27.5 us  [the longest x1 21.9 us: local(): lax.psum(jnp.sum(normalized_gradient * unit_input, axis=0), 'fs')]
where the time goes in v1:
time: 585 us
  waiting for transfers between devices  480 us (82%)
  matrix products  44.3 us (8%)
  blocking collectives  27.5 us (5%)
  between operations  14.2 us (2%)
  local copies, waits for them, and re-layouts  10.6 us (2%)
  other arithmetic  8.4 us (1%)
    reduce_scatter x1, waiting for transfers between devices, local(): lax.psum_scatter(0.5 * lax.dot_general(reordered, hidden, contract_rows,...  182 us
    all_gather x1, waiting for transfers between devices, local(): lax.all_gather(gate_weight, 'fs', axis=0, tiled=True)  95.9 us
    all_gather x1, waiting for transfers between devices, local(): lax.all_gather(up_weight, 'fs', axis=0, tiled=True)  91.2 us
    all_gather x1, waiting for transfers between devices, local(): lax.all_gather(down_weight, 'fs', axis=0, tiled=True)  84.4 us
    psum x1, waiting for transfers between devices, local(): summed_units = lax.psum(partial_value.astype(jnp.bfloat16), 'tp')  23.5 us
    psum x1, blocking collectives, local(): lax.psum(jnp.sum(normalized_gradient * unit_input, axis=0), 'fs')  21.9 us
  transfers between devices with their start and end apart: 6, of which 5 were waited for; matrix products, arithmetic and copies ran while one was open for 10% of the time, Pallas kernels for 0%

profile of v1, /device:TPU:0, one launch (start us, length us, event | category | flops | bytes accessed | tf_op | source)
XLA Modules:
  0.0 584.9 jit_solution(11957123939218448352)
XLA Ops:
  7.2 0.7 all-gather.9.cloned.1.call-update
  8.0 0.7 all-gather.7.cloned.1.call-update
  8.7 0.7 all-gather.5.cloned.1.call-update
  9.5 2.5 copy.11
  12.0 3.3 copy.12
  15.2 0.5 fusion.9
  15.7 95.9 %all-gather.9.cloned.1.call-done = bf16[2048,1536]{1,0:T(8,128)(2,1)} async-done(((bf16[256,1536]{1,0:T(8,128)(2,1)}), bf16[2048,1536]{1,0:T(8,128)(2,1)}) %all-gather.9.cloned.1.call-update) | async-done | bytes 6291472 | tf_op jit(solution)/shard_map/all_gather | solution.py:19
  111.6 7.9 %fusion.14 = f32[512,1536]{1,0:T(8,128)} fusion(bf16[2048,1536]{1,0:T(8,128)(2,1)} %all-gather.9.cloned.1.call-done, bf16[512,2048]{1,0:T(8,128)(2,1)S(1)} %copy-done, f32[2048]{0:T(1024)S(1)} %copy-done.3, f32[512]{0:T(512)S(1)} %add_rsqrt_fusion), kind=kOutput, calls=%fused_computation.25 | convolution fusion | flops 3225419776 | bytes 11544576 | tf_op jit(solution)/shard_map/dot_general | solution.py:23
  119.5 91.2 %all-gather.7.cloned.1.call-done = bf16[2048,1536]{1,0:T(8,128)(2,1)} async-done(((bf16[256,1536]{1,0:T(8,128)(2,1)}), bf16[2048,1536]{1,0:T(8,128)(2,1)}) %all-gather.7.cloned.1.call-update) | async-done | bytes 6291472 | tf_op jit(solution)/shard_map/all_gather | solution.py:20
  210.7 5.8 fusion.16
  216.5 1.7 copy-done.6
  218.2 6.9 %multiply_bitcast_fusion = f32[2048,1536]{0,1:T(8,128)} fusion(bf16[512,2048]{0,1:T(8,128)(2,1)S(1)} %bitcast.14, f32[512,1536]{1,0:T(8,128)S(1)} %fusion.16, f32[512,1536]{1,0:T(8,128)S(1)} %copy-done.4), kind=kOutput, calls=%fused_computation | convolution fusion | flops 3229089792 | bytes 20971520 | tf_op jit(solution)/shard_map/dot_general | solution.py:57
  225.2 0.2 all-reduce.2.cloned.1.call-start
  225.4 84.4 %all-gather.5.cloned.1.call-done = bf16[2048,1536]{1,0:T(8,128)(2,1)} async-done(((bf16[256,1536]{1,0:T(8,128)(2,1)}), bf16[2048,1536]{1,0:T(8,128)(2,1)}) %all-gather.5.cloned.1.call-update) | async-done | bytes 6291472 | tf_op jit(solution)/shard_map/all_gather | solution.py:21
  309.8 8.6 %convolution_multiply_fusion = f32[512,1536]{1,0:T(8,128)} fusion(bf16[512,2048]{1,0:T(8,128)(2,1)} %param.11, bf16[2048,1536]{1,0:T(8,128)(2,1)} %all-gather.5.cloned.1.call-done), kind=kOutput, calls=%fused_computation.17 | convolution fusion | flops 3222011904 | bytes 11534336 | tf_op jit(solution)/shard_map/dot_general | solution.py:25
  318.4 8.6 %fusion.12 = f32[512,2048]{1,0:T(8,128)S(1)} fusion(bf16[2048,1536]{1,0:T(8,128)(2,1)} %all-gather.9.cloned.1.call-done, f32[512,1536]{1,0:T(8,128)S(1)} %copy-done.5, f32[512,1536]{1,0:T(8,128)} %convolution_multiply_fusion, f32[512,1536]{1,0:T(8,128)S(1)} %copy-done.7), kind=kOutput, calls=%fused_computation.23 | convolution fusion | flops 3229089792 | bytes 19922944 | tf_op jit(solution)/shard_map/dot_general | solution.py:32
  327.0 6.6 %add_convert_fusion = bf16[512,2048]{1,0:T(8,128)(2,1)} fusion(f32[512,2048]{1,0:T(8,128)S(1)} %fusion.12, bf16[2048,1536]{1,0:T(8,128)(2,1)S(1)} %bitcast.16, f32[512,1536]{1,0:T(8,128)} %convolution_multiply_fusion, f32[512,1536]{1,0:T(8,128)S(1)} %copy-done.5), kind=kOutput, calls=%fused_computation.16 | convolution fusion | flops 3228041216 | bytes 18874368 | tf_op jit(solution)/shard_map/dot_general | solution.py:34
  333.7 182.4 %reduce-scatter.2.cloned.1.call-done = f32[128,1536]{0,1:T(8,128)} async-done(((f32[2048,1536]{0,1:T(8,128)}), f32[128,1536]{0,1:T(8,128)}) %reduce-scatter.2.cloned.1.call-update) | async-done | bytes 786448 | tf_op jit(solution)/shard_map/reduce_scatter | solution.py:56
  516.1 23.5 %all-reduce.2.cloned.1.call-done = bf16[512,2048]{1,0:T(8,128)(2,1)} async-done(((bf16[512,2048]{1,0:T(8,128)(2,1)}), bf16[512,2048]{1,0:T(8,128)(2,1)}) %all-reduce.2.cloned.1.call-update) | async-done | bytes 2097168 | tf_op jit(solution)/shard_map/psum | solution.py:35
  539.7 2.9 fusion.10
  542.6 21.9 %psum.22 = f32[2048]{0:T(1024)S(1)} all-reduce(f32[2048]{0:T(1024)S(1)} %get-tuple-element.12), channel_id=1, replica_groups=mesh['rep'=2,'fs'=8,'tp'=2] {'fs'}, use_global_device_ids=true, to_apply=%region_4.0 | all-reduce | flops 2048 | bytes 16384 | tf_op jit(solution)/shard_map/psum | solution.py:38
  564.5 5.6 psum.23
  570.1 5.0 fusion.6
  575.1 3.0 copy.13
  (31 shorter events, 0.3 us)
Async XLA Ops:
  7.2 2.3 copy-start.1
  7.2 104.4 %all-gather.9.cloned.1.call-start = ((), (), s32[]{:S(2)}) async-start(), calls=%async_computation.3 | async-start | bytes 7077888 | tf_op jit(solution)/shard_map/all_gather | solution.py:19
  7.9 202.8 %all-gather.7.cloned.1.call-start = ((), (), s32[]{:S(2)}) async-start(), calls=%async_computation.2 | async-start | bytes 7077888 | tf_op jit(solution)/shard_map/all_gather | solution.py:20
  8.7 301.1 %all-gather.5.cloned.1.call-start = ((), (), s32[]{:S(2)}) async-start(), calls=%async_computation.1 | async-start | bytes 7077888 | tf_op jit(solution)/shard_map/all_gather | solution.py:21
  9.4 506.7 %reduce-scatter.2.cloned.1.call-start = ((), (), s32[]{:S(2)}) async-start(), calls=%async_computation.5 | async-start | bytes 13369344 | tf_op jit(solution)/shard_map/reduce_scatter | solution.py:56
  12.0 3.3 copy-start
  12.0 99.7 %copy-start.3 = (f32[2048]{0:T(1024)S(1)}, f32[2048]{0:T(1024)}, u32[]{:S(2)}) copy-start(f32[2048]{0:T(1024)} %param.7) | copy-start | bytes 24580
  210.7 7.5 %copy-start.2 = (bf16[512,2,8,128]{0,3,2,1:T(8,128)(2,1)S(1)}, bf16[512,2,8,128]{0,3,2,1:T(8,128)(2,1)}, u32[]{:S(2)}) copy-start(bf16[512,2,8,128]{0,3,2,1:T(8,128)(2,1)} %copy.12) | copy-start | bytes 6291460
  210.7 7.5 %copy-start.4 = (f32[512,1536]{1,0:T(8,128)S(1)}, f32[512,1536]{1,0:T(8,128)}, u32[]{:S(2)}) copy-start(f32[512,1536]{1,0:T(8,128)} %fusion.14) | copy-start | bytes 9437188
  216.5 1.8 copy-start.6
  225.2 314.5 %all-reduce.2.cloned.1.call-start = ((), (), s32[]{:S(2)}) async-start(), calls=%async_computation.4 | async-start | bytes 4194304 | tf_op jit(solution)/shard_map/psum | solution.py:35
  309.8 8.6 %copy-start.5 = (f32[512,1536]{1,0:T(8,128)S(1)}, f32[512,1536]{1,0:T(8,128)}, u32[]{:S(2)}) copy-start(f32[512,1536]{1,0:T(8,128)} %fusion.14) | copy-start | bytes 9437188
  309.8 8.6 %copy-start.7 = (f32[512,1536]{1,0:T(8,128)S(1)}, f32[512,1536]{1,0:T(8,128)}, u32[]{:S(2)}) copy-start(f32[512,1536]{1,0:T(8,128)} %copy-done.6) | copy-start | bytes 9437188
  309.8 17.2 %slice-start = ((s8[6291456]{0:T(1024)(128)(4,1)}), s8[4194304]{0:T(1024)(128)(4,1)S(1)}, s32[]{:S(2)}) async-start(s8[6291456]{0:T(1024)(128)(4,1)} %bitcast.15), calls=%async_computation.7 | async-start | bytes 8388608
  318.4 8.6 %slice-start.1 = ((s8[6291456]{0:T(1024)(128)(4,1)}), s8[2097152]{0:T(1024)(128)(4,1)S(1)}, s32[]{:S(2)}) async-start(s8[6291456]{0:T(1024)(128)(4,1)} %bitcast.15), calls=%async_computation.8 | async-start | bytes 4194304
  333.6 241.4 %all-gather.11.cloned.1.call-start = ((), (), s32[]{:S(2)}) async-start(), calls=%async_computation.6 | async-start | bytes 2359296 | tf_op jit(solution)/shard_map/all_gather | solution.py:62
Sparse Core Ops, SparseCore 0:
  10.2 101.4 all-gather.8
  113.8 96.8 all-gather.6
  212.9 96.8 all-gather.4
  315.3 200.7 reduce-scatter.1
  518.9 20.7 all-reduce.1
  541.1 28.4 all-gather.10
